TPU v7x, 512 devices: a whole 4x4x16 slice. The times are simulated.
512 devices in a mesh: ep: 32 (over z, core), tp: 16 (over y, x).
Axes of the slice: x: 4, y: 4, z: 16, core: 2. Of those that a mesh axis runs over, the one named last changes fastest.
Arguments:
- queries: bfloat16 [16384, 2048], P('ep', 'tp'), may hold values from -220 to 220
- keys: bfloat16 [16384, 2048], P('ep', 'tp'), may hold values from -6 to 6
- values: bfloat16 [16384, 2048], P('ep', 'tp'), may hold values from -6 to 6
- log_gate_sums: float32 [16384, 16], P(None, 'tp'), may hold values from -16384 to 0, as said below
- mixer_weight: bfloat16 [2048, 2048], P('tp'), may hold values from -2.5 to 2.5
- moe_rows: bfloat16 [6144, 2048], P('ep'), may hold values from -6 to 6
- route_ids: int32 [6144, 2], P('ep'), may hold values from 0 to 31, all different within a row; in each aligned block of 192 rows (0 to 191, 192 to 383, ...) at most 18 rows name the same one
- group_gate: float32 [6144], P('ep'), may hold values from 0.25 to 1
- inner_gate: float32 [6144, 2], P('ep'), may hold values from 0.2 to 1
- norm_gain: float32 [2048], replicated, may hold values from 0.1 to 1.9
- gate_weight: bfloat16 [32, 2048, 4096], P('ep', None, 'tp'), may hold values from -0.125 to 0.125
- up_weight: bfloat16 [32, 2048, 4096], P('ep', None, 'tp'), may hold values from -0.125 to 0.125
- down_weight: bfloat16 [32, 4096, 2048], P('ep', 'tp'), may hold values from -0.09375 to 0.09375
Outputs:
- mixer_out: bfloat16 [16384, 2048], P('ep', 'tp')
- moe_out: bfloat16 [6144, 2048], P('ep', 'tp')
Inputs may be any that keep to these rules, and one draw needn't show every extreme that they name: `route_ids`: each row names 2 different experts; among the rows of one index of ep no expert is named more than 18 times, a bound that some block reaches. `log_gate_sums`: never rising along the positions of a head.
All inputs are finite; a program needn't handle non-finite values.
Results may differ from a plain program's by a relative error of at most 0.015.
Values may be sent and summed in bfloat16 or wider, within the bound.
A program may use at most 64 MiB of HBM per device.

v0:
```python
import jax
import jax.numpy as jnp
from jax import lax
from jax.sharding import PartitionSpec as P

LOW_SCORE = -1e30
NORM_EPS = 1e-06


def sent_together(arrays, axis, dim, along):
    widths = [a.shape[along] for a in arrays]
    both = jnp.concatenate(arrays, axis=along)
    out = lax.all_gather(both, axis, axis=dim, tiled=True)
    return tuple(jnp.split(out, [sum(widths[:k]) for k in range(1, len(widths))], axis=along))


def cut_along(x, dim, count):
    before, after = (x.shape[:dim], x.shape[dim + 1 :])
    return jnp.moveaxis(x.reshape(*before, count, -1, *after), dim, 0)


def sum_at_owner(x, axis, dim):
    tiles = cut_along(x, dim, lax.axis_size(axis))
    arrived = lax.all_to_all(tiles, axis, split_axis=0, concat_axis=0, tiled=True)
    return arrived.astype(jnp.float32).sum(axis=0)


def from_everyone(x, axis):
    copies = jnp.broadcast_to(x, (lax.axis_size(axis), *x.shape))
    return lax.all_to_all(copies, axis, split_axis=0, concat_axis=0, tiled=True)


def laid_out(tiles, dim):
    dims = list(tiles.shape[1:])
    dims[dim] *= tiles.shape[0]
    return jnp.moveaxis(tiles, 0, dim).reshape(dims)


def collect(x, axis, dim):
    tiles = from_everyone(x, axis)
    return laid_out(tiles, dim)


def attend_block(
    running,
    queries_here,
    query_gates,
    key_rows,
    value_rows,
    key_gates,
    query_pos,
    key_pos,
    inv_root,
):
    running_max, weight_sum, weighted = running
    scores = (
        jnp.einsum("qhd,khd->qhk", queries_here, key_rows, preferred_element_type=jnp.float32)
        * inv_root
    )
    scores = scores + query_gates[:, :, None] - key_gates.T[None, :, :]
    allowed = (key_pos[None, :] <= query_pos[:, None])[:, None, :]
    scores = jnp.where(allowed, scores, LOW_SCORE)
    new_max = jnp.maximum(running_max, jnp.max(scores, axis=2))
    shrink = jnp.exp(running_max - new_max)
    weights_now = jnp.where(allowed, jnp.exp(scores - new_max[:, :, None]), 0.0)
    weight_sum = weight_sum * shrink + jnp.sum(weights_now, axis=2)
    weighted = weighted * shrink[:, :, None] + jnp.einsum(
        "qhk,khd->qhd",
        weights_now.astype(jnp.bfloat16),
        value_rows,
        preferred_element_type=jnp.float32,
    )
    return (new_max, weight_sum, weighted)


def body(
    queries,
    keys,
    values,
    log_gate_sums,
    mixer_weight,
    moe_rows,
    route_ids,
    group_gate,
    inner_gate,
    norm_gain,
    gate_weight,
    up_weight,
    down_weight,
):
    row_count = queries.shape[0]
    heads_here = log_gate_sums.shape[1]
    head_width = queries.shape[1] // heads_here
    inv_root = head_width ** (-0.5)
    row_offset = lax.axis_index("ep") * row_count
    query_pos = row_offset + jnp.arange(row_count, dtype=jnp.int32)
    queries_here = queries.reshape(row_count, heads_here, head_width)
    query_gates = lax.dynamic_slice_in_dim(log_gate_sums, row_offset, row_count, 0)
    last_query = row_offset + row_count - 1
    start_state = (
        jnp.full((row_count, heads_here), LOW_SCORE, jnp.float32),
        jnp.zeros((row_count, heads_here), jnp.float32),
        jnp.zeros((row_count, heads_here, head_width), jnp.float32),
    )
    key_piece, value_piece = sent_together((keys, values), "ep", 0, 1)
    piece_rows = key_piece.shape[0]

    def key_step(block_index, partial_state):
        key_offset = block_index * row_count
        key_rows = lax.dynamic_slice_in_dim(key_piece, key_offset, row_count, 0).reshape(
            row_count, heads_here, head_width
        )
        value_rows = lax.dynamic_slice_in_dim(value_piece, key_offset, row_count, 0).reshape(
            row_count, heads_here, head_width
        )
        key_gates = lax.dynamic_slice_in_dim(log_gate_sums, key_offset, row_count, 0)
        key_pos = key_offset + jnp.arange(row_count, dtype=jnp.int32)

        def update(state_in):
            return attend_block(
                state_in,
                queries_here,
                query_gates,
                key_rows,
                value_rows,
                key_gates,
                query_pos,
                key_pos,
                inv_root,
            )

        def unchanged(state_in):
            return state_in

        return lax.cond(key_offset <= last_query, update, unchanged, partial_state)

    running_max, weight_sum, weighted = lax.fori_loop(
        0, piece_rows // row_count, key_step, start_state
    )
    attended = (
        (weighted / weight_sum[:, :, None])
        .astype(jnp.bfloat16)
        .reshape(row_count, heads_here * head_width)
    )
    partial_value = jnp.dot(attended, mixer_weight, preferred_element_type=jnp.float32).astype(
        jnp.bfloat16
    )
    partial_value = lax.optimization_barrier(partial_value).astype(jnp.float32)
    mixer_out = sum_at_owner(partial_value.astype(jnp.bfloat16), "tp", 1).astype(jnp.bfloat16)
    token_count = moe_rows.shape[0]
    top_count = route_ids.shape[1]
    model_width = moe_rows.shape[1]
    local_experts = gate_weight.shape[0]
    experts = lax.axis_size("ep") * local_experts
    capacity = 3 * token_count * top_count // (2 * experts)
    slot_count = experts * capacity
    rows_float = moe_rows.astype(jnp.float32)
    normed = (
        rows_float
        * lax.rsqrt(jnp.mean(rows_float * rows_float, axis=1, keepdims=True) + NORM_EPS)
        * norm_gain
    ).astype(jnp.bfloat16)
    route_weight = group_gate[:, None] * inner_gate / jnp.sum(inner_gate, axis=1, keepdims=True)
    onehot = (route_ids[:, :, None] == jnp.arange(experts, dtype=jnp.int32)[None, None, :]).astype(
        jnp.int32
    )
    onehot = onehot.reshape(token_count * top_count, experts)
    earlier_hits = jnp.cumsum(onehot, axis=0) - onehot
    slot_index = jnp.sum(earlier_hits * onehot, axis=1) + route_ids.reshape(-1) * capacity
    slot_hit = (slot_index[:, None] == jnp.arange(slot_count, dtype=jnp.int32)[None, :]).reshape(
        token_count, top_count, slot_count
    )
    dispatch = jnp.sum(slot_hit.astype(jnp.float32), axis=1).astype(jnp.bfloat16)
    combine = jnp.sum(jnp.where(slot_hit, route_weight[:, :, None], 0.0), axis=1)
    feature_cols = model_width // lax.axis_size("tp")
    own_features = lax.dynamic_slice_in_dim(
        normed, lax.axis_index("tp") * feature_cols, feature_cols, 1
    )
    outgoing = lax.dot_general(
        dispatch, own_features, (((0,), (0,)), ((), ())), preferred_element_type=jnp.float32
    ).astype(jnp.bfloat16)
    arrived = lax.all_to_all(outgoing, "ep", split_axis=0, concat_axis=0, tiled=True)
    sources = arrived.shape[0] // (local_experts * capacity)
    column_piece = collect(arrived, "tp", 1)
    piece_cols = column_piece.shape[1]
    piece_blocks = column_piece.reshape(sources, local_experts, capacity, piece_cols)
    gate_sum = jnp.einsum(
        "secd,edf->secf", piece_blocks, gate_weight, preferred_element_type=jnp.float32
    )
    up_sum = jnp.einsum(
        "secd,edf->secf", piece_blocks, up_weight, preferred_element_type=jnp.float32
    )
    hidden = (jax.nn.silu(gate_sum) * up_sum).astype(jnp.bfloat16)
    expert_part = jnp.einsum(
        "secf,efd->secd", hidden, down_weight, preferred_element_type=jnp.float32
    ).astype(jnp.bfloat16)
    expert_part = (
        lax.optimization_barrier(expert_part).astype(jnp.float32).reshape(slot_count, model_width)
    )
    expert_out = sum_at_owner(expert_part.astype(jnp.bfloat16), "tp", 1).astype(jnp.bfloat16)
    returned_rows = lax.all_to_all(expert_out, "ep", split_axis=0, concat_axis=0, tiled=True)
    moe_out = jnp.dot(
        combine, returned_rows.astype(jnp.float32), precision=lax.Precision.HIGHEST
    ).astype(jnp.bfloat16)
    return (mixer_out, moe_out)


def solution(mesh):
    return jax.shard_map(
        body,
        mesh=mesh,
        in_specs=(
            P("ep", "tp"),
            P("ep", "tp"),
            P("ep", "tp"),
            P(None, "tp"),
            P("tp", None),
            P("ep", None),
            P("ep", None),
            P("ep"),
            P("ep", None),
            P(),
            P("ep", None, "tp"),
            P("ep", None, "tp"),
            P("ep", "tp", None),
        ),
        out_specs=(P("ep", "tp"), P("ep", "tp")),
        check_vma=False,
    )
```

profile of v0, /device:TPU:481, one launch (start us, length us, event | category | flops | bytes accessed | tf_op | source)
XLA Modules:
  0.0 312.8 jit_solution(2155545839781961805)
XLA Ops:
  15.5 25.2 %all_to_all.39 = bf16[32,18,128]{2,1,0:T(8,128)(2,1)S(1)} all-to-all(bf16[32,18,128]{2,1,0:T(8,128)(2,1)S(1)} %all_to_all.26), channel_id=1, replica_groups=mesh['ep'=32,'tp'=16] {'ep'}, dimensions={0} | all-to-all | bytes 294912 | tf_op jit(solution)/shard_map/all_to_all | solution.py:182
  41.2 36.3 %all_to_all.40 = bf16[16,576,128]{2,1,0:T(8,128)(2,1)S(1)} all-to-all(bf16[16,576,128]{2,1,0:T(8,128)(2,1)S(1)} %broadcast_in_dim.58), channel_id=1, replica_groups=mesh['ep'=32,'tp'=16] {'tp'}, dimensions={0} | all-to-all | bytes 4718592 | tf_op jit(solution)/shard_map/all_to_all | solution.py:30
  90.3 4.0 %convert_element_type.87 = bf16[576,16,128]{2,1,0:T(8,128)(2,1)S(1)} reshape(bf16[32,1,18,2048]{3,2,0,1:T(8,128)(2,1)} %copy.55) | data formatting | bytes 4718592 | tf_op jit(solution)/shard_map/convert_element_type | solution.py:200
  96.4 3.7 %all-to-all-start.3 = ((bf16[16,576,128]{2,1,0:T(8,128)(2,1)}), bf16[16,576,128]{2,1,0:T(8,128)(2,1)S(1)}, u32[]{:S(2)}, u32[]{:S(2)}) async-start(bf16[16,576,128]{2,1,0:T(8,128)(2,1)} %copy.56), calls=%async_computation.3 | async-start | bytes 4718592 | tf_op jit(solution)/shard_map/all_to_all | solution.py:24
  101.4 26.4 %all-to-all-done.3 = bf16[16,576,128]{2,1,0:T(8,128)(2,1)S(1)} async-done(((bf16[16,576,128]{2,1,0:T(8,128)(2,1)}), bf16[16,576,128]{2,1,0:T(8,128)(2,1)S(1)}, u32[]{:S(2)}, u32[]{:S(2)}) %all-to-all-start.3) | async-done | bytes 2359328 | tf_op jit(solution)/shard_map/all_to_all | solution.py:24
  128.8 17.9 %all-to-all-start.4 = ((bf16[32,18,128]{2,1,0:T(8,128)(2,1)}), bf16[32,18,128]{2,1,0:T(8,128)(2,1)S(1)}, u32[]{:S(2)}, u32[]{:S(2)}) async-start(bf16[32,18,128]{2,1,0:T(8,128)(2,1)} %all_to_all.31), calls=%async_computation.4 | async-start | bytes 393216 | tf_op jit(solution)/shard_map/all_to_all | solution.py:201
  146.8 5.7 %fusion.42 = (bf16[16384,128]{1,0:T(8,128)(2,1)}, bf16[16384,128]{1,0:T(8,128)(2,1)}) fusion(bf16[16384,256]{1,0:T(8,128)(2,1)} %all-gather.2.cloned.1.call-done), kind=kLoop, calls=%fused_computation.71 | loop fusion | bytes 16777216 | tf_op jit(solution)/shard_map/split | solution.py:14
  152.6 118.1 %while.18 = (s32[]{:T(128)}, f32[512,1]{0,1:T(1,128)S(1)}, f32[512,1]{0,1:T(1,128)S(1)}, f32[512,1,128]{0,2,1:T(8,128)S(1)}, s32[]{:T(128)}, /*index=5*/bf16[163...) while((s32[]{:T(128)}, f32[512,1]{0,1:T(1,128)S(1)}, ...), condition=%wide.region_5.6_spmd.clone, body=%wide.region_0.5_spmd.clone.sunk | while | flops 138020864 | bytes 4127077 | solution.py:137
  152.6 3.7 %conditional.3 = ((f32[512,1]{0,1:T(1,128)S(1)}, f32[512,1]{0,1:T(1,128)S(1)}, f32[512,1,128]{0,2,1:T(8,128)S(1)})) conditional(s32[]{:T(128)} %convert_element_type.116, (f32[512,1]{0,1:T(1,128)S(1)}, f32[512,1]{0,1:T(1,128)S(1)}, f32[512,1,128]{0,2,1:T(8,128)S(1)}) %tuple.60, (s32[]{:T(128)}, s32[512]{0:T(512)S(1)}, s32[]{:T(128)}, ...), branch_computations={%region_1.0_spmd, %region_2.4_spmd} | conditional | flops 138020864 | bytes 4124758 | solution.py:135
  163.7 3.6 %conditional.3 = ((f32[512,1]{0,1:T(1,128)S(1)}, f32[512,1]{0,1:T(1,128)S(1)}, f32[512,1,128]{0,2,1:T(8,128)S(1)})) conditional(s32[]{:T(128)} %convert_element_type.116, (f32[512,1]{0,1:T(1,128)S(1)}, f32[512,1]{0,1:T(1,128)S(1)}, f32[512,1,128]{0,2,1:T(8,128)S(1)}) %tuple.60, (s32[]{:T(128)}, s32[512]{0:T(512)S(1)}, s32[]{:T(128)}, ...), branch_computations={%region_1.0_spmd, %region_2.4_spmd} | conditional | flops 138020864 | bytes 4124758 | solution.py:135
  171.1 3.6 %conditional.3 = ((f32[512,1]{0,1:T(1,128)S(1)}, f32[512,1]{0,1:T(1,128)S(1)}, f32[512,1,128]{0,2,1:T(8,128)S(1)})) conditional(s32[]{:T(128)} %convert_element_type.116, (f32[512,1]{0,1:T(1,128)S(1)}, f32[512,1]{0,1:T(1,128)S(1)}, f32[512,1,128]{0,2,1:T(8,128)S(1)}) %tuple.60, (s32[]{:T(128)}, s32[512]{0:T(512)S(1)}, s32[]{:T(128)}, ...), branch_computations={%region_1.0_spmd, %region_2.4_spmd} | conditional | flops 138020864 | bytes 4124758 | solution.py:135
  178.5 3.6 %conditional.3 = ((f32[512,1]{0,1:T(1,128)S(1)}, f32[512,1]{0,1:T(1,128)S(1)}, f32[512,1,128]{0,2,1:T(8,128)S(1)})) conditional(s32[]{:T(128)} %convert_element_type.116, (f32[512,1]{0,1:T(1,128)S(1)}, f32[512,1]{0,1:T(1,128)S(1)}, f32[512,1,128]{0,2,1:T(8,128)S(1)}) %tuple.60, (s32[]{:T(128)}, s32[512]{0:T(512)S(1)}, s32[]{:T(128)}, ...), branch_computations={%region_1.0_spmd, %region_2.4_spmd} | conditional | flops 138020864 | bytes 4124758 | solution.py:135
  185.9 3.6 %conditional.3 = ((f32[512,1]{0,1:T(1,128)S(1)}, f32[512,1]{0,1:T(1,128)S(1)}, f32[512,1,128]{0,2,1:T(8,128)S(1)})) conditional(s32[]{:T(128)} %convert_element_type.116, (f32[512,1]{0,1:T(1,128)S(1)}, f32[512,1]{0,1:T(1,128)S(1)}, f32[512,1,128]{0,2,1:T(8,128)S(1)}) %tuple.60, (s32[]{:T(128)}, s32[512]{0:T(512)S(1)}, s32[]{:T(128)}, ...), branch_computations={%region_1.0_spmd, %region_2.4_spmd} | conditional | flops 138020864 | bytes 4124758 | solution.py:135
  193.3 3.6 %conditional.3 = ((f32[512,1]{0,1:T(1,128)S(1)}, f32[512,1]{0,1:T(1,128)S(1)}, f32[512,1,128]{0,2,1:T(8,128)S(1)})) conditional(s32[]{:T(128)} %convert_element_type.116, (f32[512,1]{0,1:T(1,128)S(1)}, f32[512,1]{0,1:T(1,128)S(1)}, f32[512,1,128]{0,2,1:T(8,128)S(1)}) %tuple.60, (s32[]{:T(128)}, s32[512]{0:T(512)S(1)}, s32[]{:T(128)}, ...), branch_computations={%region_1.0_spmd, %region_2.4_spmd} | conditional | flops 138020864 | bytes 4124758 | solution.py:135
  200.6 3.6 %conditional.3 = ((f32[512,1]{0,1:T(1,128)S(1)}, f32[512,1]{0,1:T(1,128)S(1)}, f32[512,1,128]{0,2,1:T(8,128)S(1)})) conditional(s32[]{:T(128)} %convert_element_type.116, (f32[512,1]{0,1:T(1,128)S(1)}, f32[512,1]{0,1:T(1,128)S(1)}, f32[512,1,128]{0,2,1:T(8,128)S(1)}) %tuple.60, (s32[]{:T(128)}, s32[512]{0:T(512)S(1)}, s32[]{:T(128)}, ...), branch_computations={%region_1.0_spmd, %region_2.4_spmd} | conditional | flops 138020864 | bytes 4124758 | solution.py:135
  208.0 3.6 %conditional.3 = ((f32[512,1]{0,1:T(1,128)S(1)}, f32[512,1]{0,1:T(1,128)S(1)}, f32[512,1,128]{0,2,1:T(8,128)S(1)})) conditional(s32[]{:T(128)} %convert_element_type.116, (f32[512,1]{0,1:T(1,128)S(1)}, f32[512,1]{0,1:T(1,128)S(1)}, f32[512,1,128]{0,2,1:T(8,128)S(1)}) %tuple.60, (s32[]{:T(128)}, s32[512]{0:T(512)S(1)}, s32[]{:T(128)}, ...), branch_computations={%region_1.0_spmd, %region_2.4_spmd} | conditional | flops 138020864 | bytes 4124758 | solution.py:135
  215.4 3.6 %conditional.3 = ((f32[512,1]{0,1:T(1,128)S(1)}, f32[512,1]{0,1:T(1,128)S(1)}, f32[512,1,128]{0,2,1:T(8,128)S(1)})) conditional(s32[]{:T(128)} %convert_element_type.116, (f32[512,1]{0,1:T(1,128)S(1)}, f32[512,1]{0,1:T(1,128)S(1)}, f32[512,1,128]{0,2,1:T(8,128)S(1)}) %tuple.60, (s32[]{:T(128)}, s32[512]{0:T(512)S(1)}, s32[]{:T(128)}, ...), branch_computations={%region_1.0_spmd, %region_2.4_spmd} | conditional | flops 138020864 | bytes 4124758 | solution.py:135
  222.8 3.6 %conditional.3 = ((f32[512,1]{0,1:T(1,128)S(1)}, f32[512,1]{0,1:T(1,128)S(1)}, f32[512,1,128]{0,2,1:T(8,128)S(1)})) conditional(s32[]{:T(128)} %convert_element_type.116, (f32[512,1]{0,1:T(1,128)S(1)}, f32[512,1]{0,1:T(1,128)S(1)}, f32[512,1,128]{0,2,1:T(8,128)S(1)}) %tuple.60, (s32[]{:T(128)}, s32[512]{0:T(512)S(1)}, s32[]{:T(128)}, ...), branch_computations={%region_1.0_spmd, %region_2.4_spmd} | conditional | flops 138020864 | bytes 4124758 | solution.py:135
  230.1 3.6 %conditional.3 = ((f32[512,1]{0,1:T(1,128)S(1)}, f32[512,1]{0,1:T(1,128)S(1)}, f32[512,1,128]{0,2,1:T(8,128)S(1)})) conditional(s32[]{:T(128)} %convert_element_type.116, (f32[512,1]{0,1:T(1,128)S(1)}, f32[512,1]{0,1:T(1,128)S(1)}, f32[512,1,128]{0,2,1:T(8,128)S(1)}) %tuple.60, (s32[]{:T(128)}, s32[512]{0:T(512)S(1)}, s32[]{:T(128)}, ...), branch_computations={%region_1.0_spmd, %region_2.4_spmd} | conditional | flops 138020864 | bytes 4124758 | solution.py:135
  237.5 3.6 %conditional.3 = ((f32[512,1]{0,1:T(1,128)S(1)}, f32[512,1]{0,1:T(1,128)S(1)}, f32[512,1,128]{0,2,1:T(8,128)S(1)})) conditional(s32[]{:T(128)} %convert_element_type.116, (f32[512,1]{0,1:T(1,128)S(1)}, f32[512,1]{0,1:T(1,128)S(1)}, f32[512,1,128]{0,2,1:T(8,128)S(1)}) %tuple.60, (s32[]{:T(128)}, s32[512]{0:T(512)S(1)}, s32[]{:T(128)}, ...), branch_computations={%region_1.0_spmd, %region_2.4_spmd} | conditional | flops 138020864 | bytes 4124758 | solution.py:135
  244.9 3.6 %conditional.3 = ((f32[512,1]{0,1:T(1,128)S(1)}, f32[512,1]{0,1:T(1,128)S(1)}, f32[512,1,128]{0,2,1:T(8,128)S(1)})) conditional(s32[]{:T(128)} %convert_element_type.116, (f32[512,1]{0,1:T(1,128)S(1)}, f32[512,1]{0,1:T(1,128)S(1)}, f32[512,1,128]{0,2,1:T(8,128)S(1)}) %tuple.60, (s32[]{:T(128)}, s32[512]{0:T(512)S(1)}, s32[]{:T(128)}, ...), branch_computations={%region_1.0_spmd, %region_2.4_spmd} | conditional | flops 138020864 | bytes 4124758 | solution.py:135
  252.3 3.6 %conditional.3 = ((f32[512,1]{0,1:T(1,128)S(1)}, f32[512,1]{0,1:T(1,128)S(1)}, f32[512,1,128]{0,2,1:T(8,128)S(1)})) conditional(s32[]{:T(128)} %convert_element_type.116, (f32[512,1]{0,1:T(1,128)S(1)}, f32[512,1]{0,1:T(1,128)S(1)}, f32[512,1,128]{0,2,1:T(8,128)S(1)}) %tuple.60, (s32[]{:T(128)}, s32[512]{0:T(512)S(1)}, s32[]{:T(128)}, ...), branch_computations={%region_1.0_spmd, %region_2.4_spmd} | conditional | flops 138020864 | bytes 4124758 | solution.py:135
  273.3 3.7 %all-to-all-start = ((bf16[16,512,128]{2,1,0:T(8,128)(2,1)}), bf16[16,512,128]{2,1,0:T(8,128)(2,1)S(1)}, u32[]{:S(2)}, u32[]{:S(2)}) async-start(bf16[16,512,128]{2,1,0:T(8,128)(2,1)} %bitcast_bitcast_fusion), calls=%async_computation | async-start | bytes 4194304 | tf_op jit(solution)/shard_map/all_to_all | solution.py:24
  279.1 25.9 %all-to-all-done = bf16[16,512,128]{2,1,0:T(8,128)(2,1)S(1)} async-done(((bf16[16,512,128]{2,1,0:T(8,128)(2,1)}), bf16[16,512,128]{2,1,0:T(8,128)(2,1)S(1)}, u32[]{:S(2)}, u32[]{:S(2)}) %all-to-all-start) | async-done | bytes 2097184 | tf_op jit(solution)/shard_map/all_to_all | solution.py:24
  (371 shorter events, 212.0 us)
Async XLA Ops:
  7.2 79.2 %copy-start = (bf16[1,256,2048]{2,1,0:T(8,128)(2,1)S(1)}, bf16[1,256,2048]{2,1,0:T(8,128)(2,1)}, u32[]{:S(2)}) copy-start(bf16[1,256,2048]{2,1,0:T(8,128)(2,1)} %param.29) | copy-start | bytes 3145732
  7.2 6.6 %copy-start.4 = (s32[192,2]{0,1:T(2,128)S(1)}, s32[192,2]{0,1:T(2,128)}, u32[]{:S(2)}) copy-start(s32[192,2]{0,1:T(2,128)} %param.23) | copy-start | bytes 4612
  7.2 7.7 %copy-start.1 = (bf16[192,2048]{1,0:T(8,128)(2,1)S(1)}, bf16[192,2048]{1,0:T(8,128)(2,1)}, u32[]{:S(2)}) copy-start(bf16[192,2048]{1,0:T(8,128)(2,1)} %param.22) | copy-start | bytes 2359300
  7.2 6.6 %copy-start.5 = (f32[192,2]{0,1:T(2,128)S(1)}, f32[192,2]{0,1:T(2,128)}, u32[]{:S(2)}) copy-start(f32[192,2]{0,1:T(2,128)} %param.25) | copy-start | bytes 4612
  7.2 6.6 %copy-start.7 = (f32[192]{0:T(256)S(1)}, f32[192]{0:T(256)}, u32[]{:S(2)}) copy-start(f32[192]{0:T(256)} %param.24) | copy-start | bytes 2308
  7.2 139.6 %all-gather.2.cloned.1.call-start = ((), (), s32[]{:S(2)}) async-start(), calls=%async_computation.5 | async-start | bytes 8650752 | tf_op jit(solution)/shard_map/all_gather | solution.py:13
  81.8 3.3 %copy-start.2 = (bf16[32,18,2048]{2,1,0:T(8,128)(2,1)S(1)}, bf16[32,18,2048]{2,1,0:T(8,128)(2,1)}, u32[]{:S(2)}) copy-start(bf16[32,18,2048]{2,1,0:T(8,128)(2,1)} %reshape.213) | copy-start | bytes 7077892
  81.8 3.5 %copy-start.8 = (bf16[1,2048,256]{2,1,0:T(8,128)(2,1)S(1)}, bf16[1,2048,256]{2,1,0:T(8,128)(2,1)}, u32[]{:S(2)}) copy-start(bf16[1,2048,256]{2,1,0:T(8,128)(2,1)} %param.28) | copy-start | bytes 3145732
  96.4 31.4 %all-to-all-start.3 = ((bf16[16,576,128]{2,1,0:T(8,128)(2,1)}), bf16[16,576,128]{2,1,0:T(8,128)(2,1)S(1)}, u32[]{:S(2)}, u32[]{:S(2)}) async-start(bf16[16,576,128]{2,1,0:T(8,128)(2,1)} %copy.56), calls=%async_computation.3 | async-start | bytes 4718592 | tf_op jit(solution)/shard_map/all_to_all | solution.py:24
  128.8 144.5 %all-to-all-start.4 = ((bf16[32,18,128]{2,1,0:T(8,128)(2,1)}), bf16[32,18,128]{2,1,0:T(8,128)(2,1)S(1)}, u32[]{:S(2)}, u32[]{:S(2)}) async-start(bf16[32,18,128]{2,1,0:T(8,128)(2,1)} %all_to_all.31), calls=%async_computation.4 | async-start | bytes 393216 | tf_op jit(solution)/shard_map/all_to_all | solution.py:201
  146.8 5.8 %copy-start.6 = (f32[512,1]{0,1:T(1,128)S(1)}, f32[512,1]{0,1:T(1,128)}, u32[]{:S(2)}) copy-start(f32[512,1]{0,1:T(1,128)} %constant_dynamic-slice_fusion.1) | copy-start | bytes 6148
  146.8 5.8 %copy-start.9 = (bf16[512,128]{1,0:T(8,128)(2,1)S(1)}, bf16[512,128]{1,0:T(8,128)(2,1)}, u32[]{:S(2)}) copy-start(bf16[512,128]{1,0:T(8,128)(2,1)} %param.17) | copy-start | bytes 393220
  152.6 118.1 %copy-start.3 = (bf16[128,2048]{1,0:T(8,128)(2,1)S(1)}, bf16[128,2048]{1,0:T(8,128)(2,1)}, u32[]{:S(2)}) copy-start(bf16[128,2048]{1,0:T(8,128)(2,1)} %param.21) | copy-start | bytes 1572868
  273.3 31.7 %all-to-all-start = ((bf16[16,512,128]{2,1,0:T(8,128)(2,1)}), bf16[16,512,128]{2,1,0:T(8,128)(2,1)S(1)}, u32[]{:S(2)}, u32[]{:S(2)}) async-start(bf16[16,512,128]{2,1,0:T(8,128)(2,1)} %bitcast_bitcast_fusion), calls=%async_computation | async-start | bytes 4194304 | tf_op jit(solution)/shard_map/all_to_all | solution.py:24
Sparse Core Ops, SparseCore 0:
  10.2 84.1 all-gather.1
where the time goes:
time: 315 us; the launch traced here: 313 us
  matrix products  92.2 us (29%)
  blocking collectives  61.5 us (20%)
  waiting for transfers between devices  52.3 us (17%)
  local copies, waits for them, and re-layouts  48.5 us (15%)
  starting transfers between devices  25.4 us (8%)
  other arithmetic  15.4 us (5%)
  between operations  14.3 us (5%)
  loops' own time  3.22 us (1%)
    all_to_all x2, waiting for transfers between devices, sum_at_owner(): lax.all_to_all(tiles, axis, split_axis=0, concat_axis=0, tiled=True)  52.3 us
    dot_general x32, matrix products, attend_block(): jnp.einsum('qhk,khd->qhd', weights_now.astype(jnp.bfloat16), value_rows,...  42.5 us
    dot_general x32, matrix products, attend_block(): jnp.einsum('qhd,khd->qhk', queries_here, key_rows, preferred_element_type...  41.5 us
    all_to_all x1, blocking collectives, from_everyone(): return lax.all_to_all(copies, axis, split_axis=0, concat_axis=0, tiled=True)  36.3 us
    all_to_all x1, blocking collectives, body(): lax.all_to_all(outgoing, 'ep', split_axis=0, concat_axis=0, tiled=True)  25.2 us
    dynamic_slice x32, local copies, waits for them, and re-layouts, key_step(): lax.dynamic_slice_in_dim(log_gate_sums, key_offset, row_count, 0)  22.1 us
    all_to_all x1, starting transfers between devices, body(): lax.all_to_all(expert_out, 'ep', split_axis=0, concat_axis=0, tiled=True)  17.9 us
    reduce_sum x32, other arithmetic, attend_block(): weight_sum = weight_sum * shrink + jnp.sum(weights_now, axis=2)  7.68 us
  transfers between devices with their start and end apart: 4, of which 2 were waited for; matrix products, arithmetic and copies ran while one was open for 49% of the time, Pallas kernels for 0%

commit v1 on v0

v1 whole, which is shorter than its diff:
```python
import functools

import jax
import jax.numpy as jnp
from jax import lax
from jax.experimental import pallas as pl
from jax.experimental.pallas import tpu as pltpu
from jax.sharding import PartitionSpec as P

LOW_SCORE = -1e30
NORM_EPS = 1e-06
LOG2E = 1.4426950408889634
LANES = 128
MESH = pl.DeviceIdType.MESH
F32 = jnp.float32
BF16 = jnp.bfloat16


def one_hot(mask):
    return jnp.where(mask, 1.0, 0.0).astype(BF16)


class Links:

    def __init__(self, sems, limit):
        self.sems, self.limit, self.used, self.sent = sems, limit, 0, []

    def new(self):
        self.used += 1
        assert self.used <= self.limit
        return self.sems.at[self.used - 1]

    def copy(self, src, dst, device):
        c = pltpu.make_async_remote_copy(
            src_ref=src,
            dst_ref=dst,
            send_sem=self.new(),
            recv_sem=self.new(),
            device_id=device,
            device_id_type=MESH,
        )
        return c

    def start(self, c):
        c.start()
        self.sent.append(c)

    def finish(self):
        for c in self.sent:
            c.wait_send()
        self.sent = []


class GatherLine:

    def __init__(self, links, n, c, dev, block, first, second):
        self.links, self.n = links, n
        nxt, prv = (c + 1) % n, (c + n - 1) % n
        if n == 1:
            return
        self.up = links.copy(block(c), block(c), dev(nxt))
        if n == 4:
            self.down = links.copy(block(c), block(c), dev(prv))
            self.relay_up = links.copy(first(block(prv)), first(block(prv)), dev(nxt))
            self.relay_down = links.copy(second(block(nxt)), second(block(nxt)), dev(prv))

    def begin(self):
        if self.n > 1:
            self.links.start(self.up)
        if self.n == 4:
            self.links.start(self.down)

    def relay(self):
        if self.n == 4:
            self.up.wait_recv()
            self.links.start(self.relay_up)
            self.down.wait_recv()
            self.links.start(self.relay_down)

    def end(self):
        if self.n == 2:
            self.up.wait_recv()
        if self.n == 4:
            self.relay_up.wait_recv()
            self.relay_down.wait_recv()


class SumLine:

    def __init__(self, links, n, c, dev, block, first, second, half_a, half_b, full_a, full_b):
        self.links, self.n, self.c, self.block = links, n, c, block
        self.first, self.second = first, second
        self.half_a, self.half_b, self.full_a, self.full_b = half_a, half_b, full_a, full_b
        nxt, prv, far = (c + 1) % n, (c + n - 1) % n, (c + 2) % n
        self.nxt, self.prv = nxt, prv
        if n == 1:
            return
        if n == 4:
            self.far_up = links.copy(first(block(far)), half_a, dev(nxt))
            self.far_down = links.copy(second(block(far)), half_b, dev(prv))
            self.down = links.copy(block(prv), full_b, dev(prv))
        self.up = links.copy(block(nxt), full_a, dev(nxt))

    def begin(self):
        if self.n == 4:
            self.links.start(self.far_up)
            self.links.start(self.far_down)

    def relay(self):
        if self.n == 4:
            self.far_up.wait_recv()
            part = self.first(self.block(self.nxt))
            part[...] = (part[...].astype(F32) + self.half_a[...].astype(F32)).astype(BF16)
            self.links.start(self.up)
            self.far_down.wait_recv()
            part = self.second(self.block(self.prv))
            part[...] = (part[...].astype(F32) + self.half_b[...].astype(F32)).astype(BF16)
            self.links.start(self.down)
        elif self.n == 2:
            self.links.start(self.up)

    def end(self):
        total = self.block(self.c)[...].astype(F32)
        if self.n > 1:
            self.up.wait_recv()
            total = total + self.full_a[...].astype(F32)
        if self.n == 4:
            self.down.wait_recv()
            total = total + self.full_b[...].astype(F32)
        return total


class SumPlane:

    def __init__(self, links, nx, ny, x, y, at_x, at_y, part, bufs):
        rows = part.shape[2]
        h = rows // 2
        q = h // 2
        (ha, hb, fa, fb, sa, ga, gb, ea, eb) = bufs[:9]
        (hc, hd, fc, fd, sb, gc, gd, ec, ed) = bufs[9:]
        self.sa, self.sb = sa, sb

        def wide_first(r):
            return r.at[:, pl.ds(0, q), :]

        def wide_second(r):
            return r.at[:, pl.ds(q, q), :]

        def flat_first(r):
            return r.at[pl.ds(0, q), :]

        def flat_second(r):
            return r.at[pl.ds(q, q), :]

        self.a1 = SumLine(
            links, nx, x, at_x, lambda c: part.at[:, c, pl.ds(0, h), :], wide_first, wide_second, ha, hb, fa, fb
        )
        self.b1 = SumLine(
            links, ny, y, at_y, lambda c: part.at[c, :, pl.ds(h, h), :], wide_first, wide_second, hc, hd, fc, fd
        )
        self.a2 = SumLine(links, ny, y, at_y, lambda c: sa.at[c], flat_first, flat_second, ga, gb, ea, eb)
        self.b2 = SumLine(links, nx, x, at_x, lambda c: sb.at[c], flat_first, flat_second, gc, gd, ec, ed)

    def steps(self, done):
        def begin():
            self.a1.begin()
            self.b1.begin()

        def relay():
            self.a1.relay()
            self.b1.relay()

        def turn():
            self.sa[...] = self.a1.end().astype(BF16)
            self.a2.begin()
            self.sb[...] = self.b1.end().astype(BF16)
            self.b2.begin()

        def relay2():
            self.a2.relay()
            self.b2.relay()

        def end():
            done(self.a2.end(), self.b2.end())

        return [begin, relay, turn, relay2, end]


def sum_buffers(nx, ny, rows):
    h = rows // 2
    q = h // 2

    def v(*shape):
        return pltpu.VMEM((*shape, LANES), BF16)

    return [
        v(ny, q), v(ny, q), v(ny, h), v(ny, h), v(ny, h), v(q), v(q), v(h), v(h),
        v(nx, q), v(nx, q), v(nx, h), v(nx, h), v(nx, h), v(q), v(q), v(h), v(h),
    ]


SEM_LIMIT = 240


def kernel(cfg, *refs):
    (nz, nx, ny, cap, slots, moe_at) = cfg
    (q_h, k_h, v_h, gates_h, mixw_h, rows_h, rids, rids_t, weight, gain, wg_h, wu_h, wd_h) = refs[:13]
    (out_mix, out_moe) = refs[13:15]
    (
        k_all, v_all, q_v, gk, acc, top,
        mixw, mix_part, att,
        rows_v, wg, wu, wd,
        disp, arrived, feats, part, back, ret,
        sems, dsem_s, dsem_r, rsem_s, rsem_r, lsem,
    ) = refs[15:40]
    mix_bufs = refs[40:58]
    moe_bufs = refs[58:76]

    ep_n, tp_n = 2 * nz, nx * ny
    ep, tp = lax.axis_index("ep"), lax.axis_index("tp")
    z, core = ep // 2, ep % 2
    y, x = tp // nx, tp % nx
    rows_a = q_h.shape[0]
    rows_m = rows_h.shape[0]
    width = rows_h.shape[1]
    experts = ep_n
    held = experts * cap
    links = Links(sems, SEM_LIMIT)

    def at_ep(p):
        return {"ep": p}

    def at_x(c):
        return {"tp": y * nx + c}

    def at_y(c):
        return {"tp": c * nx + x}

    own_rows = pl.ds(pl.multiple_of(core * rows_a, rows_a), rows_a)

    def mine(buf, chip):
        return buf.at[chip, own_rows, :]

    loads = [
        pltpu.make_async_copy(src, dst, lsem.at[i])
        for i, (src, dst) in enumerate(
            [
                (rows_h, rows_v),
                (k_h, mine(k_all, z)),
                (v_h, mine(v_all, z)),
                (q_h, q_v),
                (gates_h, gk),
                (wg_h, wg),
                (wu_h, wu),
                (wd_h, wd),
                (mixw_h, mixw),
            ]
        )
    ]
    for c in loads:
        c.start()

    barrier = pltpu.get_barrier_semaphore()

    def greet(o, carry):
        pl.semaphore_signal(barrier, inc=1, device_id=at_ep((ep + o) % ep_n), device_id_type=MESH)
        return carry

    lax.fori_loop(1, ep_n, greet, 0)
    for o in range(1, nx):
        pl.semaphore_signal(barrier, inc=1, device_id=at_x((x + o) % nx), device_id_type=MESH)
    for o in range(1, ny):
        pl.semaphore_signal(barrier, inc=1, device_id=at_y((y + o) % ny), device_id_type=MESH)

    loads[0].wait()
    ids_t = rids_t[...].astype(F32)
    expert_rows = lax.broadcasted_iota(jnp.int32, (experts, rows_m), 0).astype(F32)
    hit0, hit1 = ids_t[0:1] == expert_rows, ids_t[1:2] == expert_rows
    before = one_hot(
        lax.broadcasted_iota(jnp.int32, (rows_m, rows_m), 0)
        < lax.broadcasted_iota(jnp.int32, (rows_m, rows_m), 1)
    )
    rank = jnp.dot(one_hot(hit0 | hit1), before, preferred_element_type=F32)
    slot0 = ids_t[0:1] * slots + jnp.sum(jnp.where(hit0, rank, 0.0), axis=0, keepdims=True)
    slot1 = ids_t[1:2] * slots + jnp.sum(jnp.where(hit1, rank, 0.0), axis=0, keepdims=True)
    slot_rows = lax.broadcasted_iota(jnp.int32, (experts * slots, rows_m), 0).astype(F32)
    select = one_hot((slot_rows == slot0) | (slot_rows == slot1))
    squares = jnp.zeros((rows_m, LANES), F32)
    for b in range(width // LANES):
        r = rows_v[:, b * LANES : (b + 1) * LANES].astype(F32)
        squares = squares + r * r
    mean = jnp.sum(squares, axis=1, keepdims=True) / width
    own_cols = pl.ds(pl.multiple_of(tp * LANES, LANES), LANES)
    normed = (rows_v[:, own_cols].astype(F32) * lax.rsqrt(mean + NORM_EPS) * gain[:, own_cols]).astype(BF16)
    disp[...] = (
        jnp.dot(select, normed, preferred_element_type=F32).astype(BF16).reshape(experts, slots, LANES)
    )

    loads[1].wait()
    loads[2].wait()
    pl.semaphore_wait(barrier, ep_n - 1 + nx - 1 + ny - 1)

    def dispatch_copy(o):
        peer = (ep + o) % ep_n
        return pltpu.make_async_remote_copy(
            src_ref=disp.at[peer],
            dst_ref=arrived.at[ep],
            send_sem=dsem_s.at[o],
            recv_sem=dsem_r.at[o],
            device_id=at_ep(peer),
            device_id_type=MESH,
        )

    def return_copy(o):
        peer = (ep + o) % ep_n
        return pltpu.make_async_remote_copy(
            src_ref=back.at[peer],
            dst_ref=ret.at[ep],
            send_sem=rsem_s.at[o],
            recv_sem=rsem_r.at[o],
            device_id=at_ep(peer),
            device_id_type=MESH,
        )

    def each_peer(do):
        def step(o, carry):
            do(o)
            return carry

        lax.fori_loop(1, ep_n, step, 0)

    each_peer(lambda o: dispatch_copy(o).start())

    up_chip = at_ep(((z + 1) % nz) * 2 + core)
    down_chip = at_ep(((z + nz - 1) % nz) * 2 + core)
    partner = at_ep(z * 2 + 1 - core)
    half = nz // 2
    reach = {"k_up": half, "k_down": half - 1, "v_up": half - 1, "v_down": half}
    ring, cross = {}, {}
    for kind in ("k", "v"):
        buf = k_all if kind == "k" else v_all
        cross[kind, 0] = links.copy(mine(buf, z), mine(buf, z), partner)
        for way, sign, dev in (("up", -1, up_chip), ("down", 1, down_chip)):
            for d in range(1, reach[kind + "_" + way] + 1):
                sent = (z + sign * (d - 1) + nz) % nz
                got = (z + sign * d + nz) % nz
                ring[kind, way, d] = links.copy(mine(buf, sent), mine(buf, sent), dev)
                cross[kind, way, d] = links.copy(mine(buf, got), mine(buf, got), partner)

    for kind in ("k", "v"):
        for way in ("up", "down"):
            if (kind, way, 1) in ring:
                links.start(ring[kind, way, 1])
        links.start(cross[kind, 0])

    arrived[ep] = disp[ep]

    scale = LOG2E * LANES**-0.5
    chunk = 2 * rows_a
    q_block = min(256, rows_a)
    top[...] = jnp.full(top.shape, LOW_SCORE, F32)
    acc[...] = jnp.zeros(acc.shape, F32)
    loads[3].wait()
    loads[4].wait()
    base = jnp.max(gk[pl.ds(z, 1), own_rows], axis=1, keepdims=True)

    def attend(chip, masked):
        bias = (gk[pl.ds(chip, 1), :] - base) * LOG2E
        ones = jnp.ones((chunk, LANES), BF16)
        for i in range(rows_a // q_block):
            here = pl.ds(i * q_block, q_block)
            scores = (
                lax.dot_general(
                    q_v[here, :], k_all[chip], (((1,), (1,)), ((), ())), preferred_element_type=F32
                )
                * scale
                - bias
            )
            if masked:
                key_pos = lax.broadcasted_iota(jnp.int32, (q_block, chunk), 1)
                query_pos = lax.broadcasted_iota(jnp.int32, (q_block, chunk), 0) + core * rows_a + i * q_block
                scores = jnp.where(key_pos <= query_pos, scores, LOW_SCORE)
            old = top[here, :]
            new = jnp.maximum(old, jnp.max(scores, axis=1, keepdims=True))
            top[here, :] = new
            shrink = jnp.exp2(old - new)
            weights = jnp.exp2(scores - new[:, 0:1]).astype(BF16)
            both = jnp.concatenate([v_all[chip], ones], axis=1)
            add = jnp.dot(weights, both, preferred_element_type=F32)
            acc[here, :] = acc[here, :] * jnp.concatenate([shrink, shrink], axis=1) + add

    gather = {}
    h, qtr = held // 2, held // 4
    gather["a1"] = GatherLine(
        links, nx, x, at_x, lambda c: feats.at[y, c, pl.ds(0, h), :],
        lambda r: r.at[pl.ds(0, qtr), :], lambda r: r.at[pl.ds(qtr, qtr), :],
    )
    gather["b1"] = GatherLine(
        links, ny, y, at_y, lambda c: feats.at[c, x, pl.ds(h, h), :],
        lambda r: r.at[pl.ds(0, qtr), :], lambda r: r.at[pl.ds(qtr, qtr), :],
    )
    gather["a2"] = GatherLine(
        links, ny, y, at_y, lambda c: feats.at[c, :, pl.ds(0, h), :],
        lambda r: r.at[:, pl.ds(0, qtr), :], lambda r: r.at[:, pl.ds(qtr, qtr), :],
    )
    gather["b2"] = GatherLine(
        links, nx, x, at_x, lambda c: feats.at[:, c, pl.ds(h, h), :],
        lambda r: r.at[:, pl.ds(0, qtr), :], lambda r: r.at[:, pl.ds(qtr, qtr), :],
    )

    def packed_row(shape, dim):
        i = lax.broadcasted_iota(jnp.int32, shape, dim)
        return (i // cap) * slots + i % cap

    def moe_arrive():
        each_peer(lambda o: dispatch_copy(o).wait_recv())
        where_from = packed_row((held, 1), 0)
        pick = one_hot(where_from == lax.broadcasted_iota(jnp.int32, (held, experts * slots), 1))
        feats[y, x] = jnp.dot(
            pick, arrived[...].reshape(experts * slots, LANES), preferred_element_type=F32
        ).astype(BF16)
        gather["a1"].begin()
        gather["b1"].begin()

    def moe_gather_relay():
        gather["a1"].relay()
        gather["b1"].relay()

    def moe_gather_turn():
        gather["a1"].end()
        gather["a2"].begin()
        gather["b1"].end()
        gather["b2"].begin()

    def moe_gather_relay2():
        gather["a2"].relay()
        gather["b2"].relay()

    made = {}

    def moe_hidden():
        gather["a2"].end()
        gather["b2"].end()
        loads[5].wait()
        loads[6].wait()
        gate, up = 0.0, 0.0
        for yy in range(ny):
            block = jnp.concatenate([feats[yy, xx] for xx in range(nx)], axis=1)
            cols = slice(yy * nx * LANES, (yy + 1) * nx * LANES)
            gate = gate + jnp.dot(block, wg[cols, :], preferred_element_type=F32)
            up = up + jnp.dot(block, wu[cols, :], preferred_element_type=F32)
        made["hidden"] = (gate / (1.0 + jnp.exp(-gate)) * up).astype(BF16)

    def project(rows, weights_ref, dest):
        for b in range(0, tp_n, 2):
            both = jnp.dot(rows, weights_ref[:, b * LANES : (b + 2) * LANES], preferred_element_type=F32)
            for e in (0, 1):
                dest[(b + e) // nx, (b + e) % nx] = both[:, e * LANES : (e + 1) * LANES].astype(BF16)

    def expert_done(first, second):
        packed = jnp.concatenate([first, second], axis=0).astype(BF16)
        where_to = packed_row((1, held), 1)
        spread = one_hot(lax.broadcasted_iota(jnp.int32, (experts * slots, held), 0) == where_to)
        back[...] = (
            jnp.dot(spread, packed, preferred_element_type=F32).astype(BF16).reshape(experts, slots, LANES)
        )
        each_peer(lambda o: return_copy(o).start())
        ret[ep] = back[ep]

    expert_sum = SumPlane(links, nx, ny, x, y, at_x, at_y, part, moe_bufs).steps(expert_done)

    def moe_down():
        loads[7].wait()
        project(made["hidden"], wd, part)
        expert_sum[0]()

    def moe_combine():
        each_peer(lambda o: return_copy(o).wait_recv())
        ids = rids[...].astype(F32)
        expert_cols = lax.broadcasted_iota(jnp.int32, (rows_m, experts), 1).astype(F32)
        hits = [ids[:, k : k + 1] == expert_cols for k in (0, 1)]
        after = one_hot(
            lax.broadcasted_iota(jnp.int32, (rows_m, rows_m), 0)
            > lax.broadcasted_iota(jnp.int32, (rows_m, rows_m), 1)
        )
        ranks = jnp.dot(after, one_hot(hits[0] | hits[1]), preferred_element_type=F32)
        slot_cols = lax.broadcasted_iota(jnp.int32, (rows_m, experts * slots), 1).astype(F32)
        rows = ret[...].reshape(experts * slots, LANES)
        total = 0.0
        for k in (0, 1):
            slot = ids[:, k : k + 1] * slots + jnp.sum(jnp.where(hits[k], ranks, 0.0), axis=1, keepdims=True)
            picked = jnp.dot(one_hot(slot_cols == slot), rows, preferred_element_type=F32)
            total = total + weight[:, k : k + 1] * picked
        out_moe[...] = total.astype(BF16)

    moe = [
        moe_arrive,
        moe_gather_relay,
        moe_gather_turn,
        moe_gather_relay2,
        lambda: (moe_hidden(), moe_down()),
        expert_sum[1],
        expert_sum[2],
        expert_sum[3],
        expert_sum[4],
        moe_combine,
    ]

    def moe_slot(number):
        while moe_at and moe and moe_at[0] <= number:
            moe_at.pop(0)
            moe.pop(0)()

    moe_at = list(moe_at)

    cross["k", 0].wait_recv()
    cross["v", 0].wait_recv()
    attend(z, True)

    def pass_on(kind, d):
        for way in ("up", "down"):
            if (kind, way, d) in ring:
                ring[kind, way, d].wait_recv()
                if (kind, way, d + 1) in ring:
                    links.start(ring[kind, way, d + 1])
                links.start(cross[kind, way, d])

    def landed(d):
        for kind in ("k", "v"):
            for way in ("up", "down"):
                if (kind, way, d) in ring:
                    cross[kind, way, d].wait_recv()

    def attend_up(d):
        @pl.when(z >= d)
        def _():
            attend(z - d, False)

    def attend_down(d):
        @pl.when(z + d >= nz)
        def _():
            attend(z + d - nz, False)

    for d in range(1, half + 1):
        pass_on("k", d)
        if d > 1:
            landed(d - 1)
            attend_up(d - 1)
        moe_slot(2 * d - 1)
        pass_on("v", d)
        if d > 1:
            attend_down(d - 1)
        moe_slot(2 * d)
    landed(half)
    attend_up(half)

    @pl.when(z < half)
    def _():
        pass

    att[...] = (acc[:, 0:LANES] / acc[:, LANES:]).astype(BF16)

    def mix_done(first, second):
        out_mix[pl.ds(0, rows_a // 2), :] = first.astype(BF16)
        out_mix[pl.ds(rows_a // 2, rows_a // 2), :] = second.astype(BF16)

    mix = SumPlane(links, nx, ny, x, y, at_x, at_y, mix_part, mix_bufs).steps(mix_done)
    loads[8].wait()
    project(att[...], mixw, mix_part)
    mix.pop(0)()
    while mix or moe:
        if moe:
            moe.pop(0)()
        if mix:
            mix.pop(0)()
    links.finish()
    each_peer(lambda o: dispatch_copy(o).wait_send())
    each_peer(lambda o: return_copy(o).wait_send())


def body(sizes, moe_at, queries, keys, values, log_gate_sums, mixer_weight, moe_rows, route_ids,
         group_gate, inner_gate, norm_gain, gate_weight, up_weight, down_weight):
    nz, nx, ny = sizes
    rows_a, rows_m, width = queries.shape[0], moe_rows.shape[0], moe_rows.shape[1]
    experts = 2 * nz
    cap = 3 * rows_m * route_ids.shape[1] // (2 * experts)
    slots = -(-cap // 16) * 16
    hidden = gate_weight.shape[2]
    held = experts * cap
    route_weight = group_gate[:, None] * inner_gate / jnp.sum(inner_gate, axis=1, keepdims=True)
    gates = log_gate_sums.reshape(nz, 2 * rows_a)

    def v(*shape, dtype=BF16):
        return pltpu.VMEM(shape, dtype)

    scratch = [
        v(nz, 2 * rows_a, LANES), v(nz, 2 * rows_a, LANES), v(rows_a, LANES), v(nz, 2 * rows_a, dtype=F32),
        v(rows_a, 2 * LANES, dtype=F32), v(rows_a, LANES, dtype=F32),
        v(LANES, width), v(ny, nx, rows_a, LANES), v(rows_a, LANES),
        v(rows_m, width), v(width, hidden), v(width, hidden), v(hidden, width),
        v(experts, slots, LANES), v(experts, slots, LANES), v(ny, nx, held, LANES), v(ny, nx, held, LANES),
        v(experts, slots, LANES), v(experts, slots, LANES),
        pltpu.SemaphoreType.DMA((SEM_LIMIT,)),
        pltpu.SemaphoreType.DMA((2 * nz,)), pltpu.SemaphoreType.DMA((2 * nz,)),
        pltpu.SemaphoreType.DMA((2 * nz,)), pltpu.SemaphoreType.DMA((2 * nz,)),
        pltpu.SemaphoreType.DMA((9,)),
        *sum_buffers(nx, ny, rows_a),
        *sum_buffers(nx, ny, held),
    ]
    hbm = pl.BlockSpec(memory_space=pl.ANY)
    vm = pl.BlockSpec(memory_space=pltpu.VMEM)
    return pl.pallas_call(
        functools.partial(kernel, (nz, nx, ny, cap, slots, moe_at)),
        out_shape=(
            jax.ShapeDtypeStruct((rows_a, LANES), BF16),
            jax.ShapeDtypeStruct((rows_m, LANES), BF16),
        ),
        in_specs=[hbm] * 6 + [vm] * 4 + [hbm] * 3,
        out_specs=(vm, vm),
        scratch_shapes=scratch,
        compiler_params=pltpu.CompilerParams(
            collective_id=0, has_side_effects=True, vmem_limit_bytes=60 * 1024 * 1024
        ),
        name="step",
    )(
        queries, keys, values, gates, mixer_weight, moe_rows, route_ids, route_ids.T, route_weight,
        norm_gain.reshape(1, -1), gate_weight[0], up_weight[0], down_weight[0],
    )


MOE_AT = (5, 6, 7, 9, 11, 14, 16)


def plane_of(tp):
    side = 1
    while side * side < tp:
        side *= 2
    return side, tp // side


def solution(mesh, plane=None, moe_at=MOE_AT):
    nx, ny = plane or plane_of(mesh.shape["tp"])
    sizes = (mesh.shape["ep"] // 2, nx, ny)
    return jax.shard_map(
        functools.partial(body, sizes, moe_at),
        mesh=mesh,
        in_specs=(
            P("ep", "tp"),
            P("ep", "tp"),
            P("ep", "tp"),
            P(None, "tp"),
            P("tp", None),
            P("ep", None),
            P("ep", None),
            P("ep"),
            P("ep", None),
            P(),
            P("ep", None, "tp"),
            P("ep", None, "tp"),
            P("ep", "tp", None),
        ),
        out_specs=(P("ep", "tp"), P("ep", "tp")),
        check_vma=False,
    )
```

time: 315 us -> 122 us (0.39)
  the two profiles are of different devices: /device:TPU:481 before, /device:TPU:1 now
where the time goes in v1:
time: 122 us; the launch traced here: 121 us
  Pallas kernels  113 us (93%)
  local copies, waits for them, and re-layouts  4.92 us (4%)
  other arithmetic  2.39 us (2%)
    pallas_call x1, Pallas kernels, body(): pl.pallas_call(functools.partial(kernel, (nz, nx, ny, cap, slots, moe_at)...  113 us
    unnamed x12, local copies, waits for them, and re-layouts  4.17 us

profile of v1, /device:TPU:1, one launch (start us, length us, event | category | flops | bytes accessed | tf_op | source)
XLA Modules:
  0.0 121.2 jit_solution(8185803881642664663)
XLA Ops:
  0.6 0.0 copy-start.2
  0.6 0.0 copy-start.3
  0.6 0.7 copy-done.2
  1.3 0.0 copy-done.3
  1.3 0.5 broadcast.5
  1.9 1.6 %reduce.3 = f32[16384]{0:T(1024)S(1)} reduce(f32[16384,1]{0,1:T(1,128)} %param.16, f32[]{:T(128)} %broadcast.5), dimensions={1}, to_apply=%param.16.reduce_sub_computation.3 | reduce | bytes 131076 | tf_op args[3]
  3.5 0.6 reshape.12.refs_3_
  4.1 0.1 copy.18
  4.3 0.0 copy-start.1
  4.3 0.7 broadcast_divide_fusion.refs_8_
  5.0 0.0 copy-done.1
  5.0 0.8 copy.20.refs_6_
  5.8 113.2 %step.1 = (bf16[512,128]{1,0:T(8,128)(2,1)}, bf16[192,128]{1,0:T(8,128)(2,1)}) custom-call(bf16[512,128]{1,0:T(8,128)(2,1)} %refs_0_.1, bf16[512,128]{1,0:T(8,128)(2,1)} %refs_1_.1, bf16[512,128]{1,0:T(8,128)(2,1)} %refs_2_.1, f32[16,1024]{1,0:T(8,128)} %reshape.12.refs_3_, bf16[128,2048]{1,0:T(8,128)(2,1)} %refs_4_.1, bf16[192,2048]{1,0:T(8,128)(2,1)} %refs_5_.1, ...), custom_call_target="tpu_custom_call" | custom-call | tf_op jit(solution)/shard_map/step/pallas_call | solution.py:612
  119.0 0.0 copy-start
  119.0 1.6 %copy.23 = bf16[512,128]{1,0:T(8,128)(2,1)} copy(bf16[512,128]{1,0:T(8,128)(2,1)} %get-tuple-element.6) | data formatting | bytes 262144
  120.6 0.0 copy-done
  120.6 0.6 copy.24
  (1 shorter events, 0.0 us)
Async XLA Ops:
  0.6 0.7 copy-start.2
  0.6 0.7 copy-start.3
  4.3 0.7 copy-start.1
  119.0 1.6 %copy-start = (bf16[192,128]{1,0:T(8,128)(2,1)S(1)}, bf16[192,128]{1,0:T(8,128)(2,1)}, u32[]{:S(2)}) copy-start(bf16[192,128]{1,0:T(8,128)(2,1)} %get-tuple-element.7) | copy-start | bytes 147460

commit v2 on v1

--- a/solution.py
+++ b/solution.py
@@ -58,29 +58,39 @@
         nxt, prv = (c + 1) % n, (c + n - 1) % n
         if n == 1:
             return
-        self.up = links.copy(block(c), block(c), dev(nxt))
+
+        def same(ref, to):
+            return links.copy(ref, ref, dev(to))
+
+        self.up = [same(first(block(c)), nxt), same(second(block(c)), nxt)]
+        self.down = []
         if n == 4:
-            self.down = links.copy(block(c), block(c), dev(prv))
-            self.relay_up = links.copy(first(block(prv)), first(block(prv)), dev(nxt))
-            self.relay_down = links.copy(second(block(nxt)), second(block(nxt)), dev(prv))
+            self.down = [same(second(block(c)), prv), same(first(block(c)), prv)]
+            self.relay_up = same(first(block(prv)), nxt)
+            self.relay_down = same(second(block(nxt)), prv)
 
     def begin(self):
-        if self.n > 1:
-            self.links.start(self.up)
-        if self.n == 4:
-            self.links.start(self.down)
+        if self.n == 1:
+            return
+        for k in (0, 1):
+            self.links.start(self.up[k])
+            if self.n == 4:
+                self.links.start(self.down[k])
 
     def relay(self):
         if self.n == 4:
-            self.up.wait_recv()
+            self.up[0].wait_recv()
             self.links.start(self.relay_up)
-            self.down.wait_recv()
+            self.down[0].wait_recv()
             self.links.start(self.relay_down)
 
     def end(self):
         if self.n == 2:
-            self.up.wait_recv()
+            self.up[0].wait_recv()
+            self.up[1].wait_recv()
         if self.n == 4:
+            self.up[1].wait_recv()
+            self.down[1].wait_recv()
             self.relay_up.wait_recv()
             self.relay_down.wait_recv()
 
@@ -98,13 +108,20 @@
         if n == 4:
             self.far_up = links.copy(first(block(far)), half_a, dev(nxt))
             self.far_down = links.copy(second(block(far)), half_b, dev(prv))
-            self.down = links.copy(block(prv), full_b, dev(prv))
-        self.up = links.copy(block(nxt), full_a, dev(nxt))
+            self.down_plain = links.copy(first(block(prv)), first(full_b), dev(prv))
+            self.down = links.copy(second(block(prv)), second(full_b), dev(prv))
+        self.up_plain = links.copy(second(block(nxt)), second(full_a), dev(nxt))
+        self.up = links.copy(first(block(nxt)), first(full_a), dev(nxt))
 
     def begin(self):
         if self.n == 4:
             self.links.start(self.far_up)
             self.links.start(self.far_down)
+            self.links.start(self.up_plain)
+            self.links.start(self.down_plain)
+        elif self.n == 2:
+            self.links.start(self.up_plain)
+            self.links.start(self.up)
 
     def relay(self):
         if self.n == 4:
@@ -116,15 +133,15 @@
             part = self.second(self.block(self.prv))
             part[...] = (part[...].astype(F32) + self.half_b[...].astype(F32)).astype(BF16)
             self.links.start(self.down)
-        elif self.n == 2:
-            self.links.start(self.up)
 
     def end(self):
         total = self.block(self.c)[...].astype(F32)
         if self.n > 1:
+            self.up_plain.wait_recv()
             self.up.wait_recv()
             total = total + self.full_a[...].astype(F32)
         if self.n == 4:
+            self.down_plain.wait_recv()
             self.down.wait_recv()
             total = total + self.full_b[...].astype(F32)
         return total
@@ -199,22 +216,22 @@
     ]
 
 
-SEM_LIMIT = 240
+SEM_LIMIT = 300
 
 
 def kernel(cfg, *refs):
     (nz, nx, ny, cap, slots, moe_at) = cfg
-    (q_h, k_h, v_h, gates_h, mixw_h, rows_h, rids, rids_t, weight, gain, wg_h, wu_h, wd_h) = refs[:13]
+    (q_h, k_h, v_h, gates_h, mixw_h, rows_h, rids_t, group_t, inner_t, gain, wg_h, wu_h, wd_h) = refs[:13]
     (out_mix, out_moe) = refs[13:15]
     (
         k_all, v_all, q_v, gk, acc, top,
         mixw, mix_part, att,
         rows_v, wg, wu, wd,
-        disp, arrived, feats, part, back, ret,
+        disp, arrived, feats, part, back, ret, table,
         sems, dsem_s, dsem_r, rsem_s, rsem_r, lsem,
-    ) = refs[15:40]
-    mix_bufs = refs[40:58]
-    moe_bufs = refs[58:76]
+    ) = refs[15:41]
+    mix_bufs = refs[41:59]
+    moe_bufs = refs[59:77]
 
     ep_n, tp_n = 2 * nz, nx * ny
     ep, tp = lax.axis_index("ep"), lax.axis_index("tp")
@@ -260,6 +277,11 @@
     for c in loads:
         c.start()
 
+    if cap % 16:
+        whole = cap // 16 * 16
+        arrived[:, whole:, :] = jnp.zeros((experts, slots - whole, LANES), BF16)
+        ret[:, whole:, :] = jnp.zeros((experts, slots - whole, LANES), BF16)
+
     barrier = pltpu.get_barrier_semaphore()
 
     def greet(o, carry):
@@ -272,6 +294,7 @@
     for o in range(1, ny):
         pl.semaphore_signal(barrier, inc=1, device_id=at_y((y + o) % ny), device_id_type=MESH)
 
+    table[...] = jnp.zeros(table.shape, F32)
     loads[0].wait()
     ids_t = rids_t[...].astype(F32)
     expert_rows = lax.broadcasted_iota(jnp.int32, (experts, rows_m), 0).astype(F32)
@@ -283,6 +306,10 @@
     rank = jnp.dot(one_hot(hit0 | hit1), before, preferred_element_type=F32)
     slot0 = ids_t[0:1] * slots + jnp.sum(jnp.where(hit0, rank, 0.0), axis=0, keepdims=True)
     slot1 = ids_t[1:2] * slots + jnp.sum(jnp.where(hit1, rank, 0.0), axis=0, keepdims=True)
+    gates_in = inner_t[...]
+    share = group_t[...] * gates_in / jnp.sum(gates_in, axis=0, keepdims=True)
+    for k, row in enumerate((slot0, slot1, share[0:1], share[1:2])):
+        table[k : k + 1, 0:rows_m] = row
     slot_rows = lax.broadcasted_iota(jnp.int32, (experts * slots, rows_m), 0).astype(F32)
     select = one_hot((slot_rows == slot0) | (slot_rows == slot1))
     squares = jnp.zeros((rows_m, LANES), F32)
@@ -300,11 +327,13 @@
     loads[2].wait()
     pl.semaphore_wait(barrier, ep_n - 1 + nx - 1 + ny - 1)
 
+    used = pl.ds(0, cap)
+
     def dispatch_copy(o):
         peer = (ep + o) % ep_n
         return pltpu.make_async_remote_copy(
-            src_ref=disp.at[peer],
-            dst_ref=arrived.at[ep],
+            src_ref=disp.at[peer, used, :],
+            dst_ref=arrived.at[ep, used, :],
             send_sem=dsem_s.at[o],
             recv_sem=dsem_r.at[o],
             device_id=at_ep(peer),
@@ -314,8 +343,8 @@
     def return_copy(o):
         peer = (ep + o) % ep_n
         return pltpu.make_async_remote_copy(
-            src_ref=back.at[peer],
-            dst_ref=ret.at[ep],
+            src_ref=back.at[peer, used, :],
+            dst_ref=ret.at[ep, used, :],
             send_sem=rsem_s.at[o],
             recv_sem=rsem_r.at[o],
             device_id=at_ep(peer),
@@ -355,6 +384,9 @@
 
     arrived[ep] = disp[ep]
 
+    def gates_of(chip, start, size):
+        return gk[:, pl.ds(pl.multiple_of(chip * 2 * rows_a + start, rows_a), size)]
+
     scale = LOG2E * LANES**-0.5
     chunk = 2 * rows_a
     q_block = min(256, rows_a)
@@ -362,10 +394,10 @@
     acc[...] = jnp.zeros(acc.shape, F32)
     loads[3].wait()
     loads[4].wait()
-    base = jnp.max(gk[pl.ds(z, 1), own_rows], axis=1, keepdims=True)
+    base = jnp.max(gates_of(z, core * rows_a, rows_a), axis=1, keepdims=True)
 
     def attend(chip, masked):
-        bias = (gk[pl.ds(chip, 1), :] - base) * LOG2E
+        bias = (gates_of(chip, 0, chunk) - base) * LOG2E
         ones = jnp.ones((chunk, LANES), BF16)
         for i in range(rows_a // q_block):
             here = pl.ds(i * q_block, q_block)
@@ -436,23 +468,27 @@
         gather["a2"].relay()
         gather["b2"].relay()
 
-    made = {}
-
-    def moe_hidden():
+    made = {"gate": 0.0, "up": 0.0}
+
+    def moe_gathered():
         gather["a2"].end()
         gather["b2"].end()
         loads[5].wait()
         loads[6].wait()
-        gate, up = 0.0, 0.0
-        for yy in range(ny):
+
+    def moe_hidden(part_rows):
+        for yy in part_rows:
             block = jnp.concatenate([feats[yy, xx] for xx in range(nx)], axis=1)
             cols = slice(yy * nx * LANES, (yy + 1) * nx * LANES)
-            gate = gate + jnp.dot(block, wg[cols, :], preferred_element_type=F32)
-            up = up + jnp.dot(block, wu[cols, :], preferred_element_type=F32)
-        made["hidden"] = (gate / (1.0 + jnp.exp(-gate)) * up).astype(BF16)
-
-    def project(rows, weights_ref, dest):
-        for b in range(0, tp_n, 2):
+            made["gate"] = made["gate"] + jnp.dot(block, wg[cols, :], preferred_element_type=F32)
+            made["up"] = made["up"] + jnp.dot(block, wu[cols, :], preferred_element_type=F32)
+
+    def moe_act():
+        gate = made["gate"]
+        made["hidden"] = (gate / (1.0 + jnp.exp(-gate)) * made["up"]).astype(BF16)
+
+    def project(rows, weights_ref, dest, start=0, stop=tp_n):
+        for b in range(start, stop, 2):
             both = jnp.dot(rows, weights_ref[:, b * LANES : (b + 2) * LANES], preferred_element_type=F32)
             for e in (0, 1):
                 dest[(b + e) // nx, (b + e) % nx] = both[:, e * LANES : (e + 1) * LANES].astype(BF16)
@@ -469,49 +505,43 @@
 
     expert_sum = SumPlane(links, nx, ny, x, y, at_x, at_y, part, moe_bufs).steps(expert_done)
 
-    def moe_down():
-        loads[7].wait()
-        project(made["hidden"], wd, part)
-        expert_sum[0]()
+    def moe_down(start, stop):
+        project(made["hidden"], wd, part, start, stop)
 
     def moe_combine():
         each_peer(lambda o: return_copy(o).wait_recv())
-        ids = rids[...].astype(F32)
-        expert_cols = lax.broadcasted_iota(jnp.int32, (rows_m, experts), 1).astype(F32)
-        hits = [ids[:, k : k + 1] == expert_cols for k in (0, 1)]
-        after = one_hot(
-            lax.broadcasted_iota(jnp.int32, (rows_m, rows_m), 0)
-            > lax.broadcasted_iota(jnp.int32, (rows_m, rows_m), 1)
-        )
-        ranks = jnp.dot(after, one_hot(hits[0] | hits[1]), preferred_element_type=F32)
+        columns = table[...].T[0:rows_m]
         slot_cols = lax.broadcasted_iota(jnp.int32, (rows_m, experts * slots), 1).astype(F32)
         rows = ret[...].reshape(experts * slots, LANES)
         total = 0.0
         for k in (0, 1):
-            slot = ids[:, k : k + 1] * slots + jnp.sum(jnp.where(hits[k], ranks, 0.0), axis=1, keepdims=True)
-            picked = jnp.dot(one_hot(slot_cols == slot), rows, preferred_element_type=F32)
-            total = total + weight[:, k : k + 1] * picked
+            hit = one_hot(slot_cols == columns[:, k : k + 1])
+            total = total + columns[:, k + 2 : k + 3] * jnp.dot(hit, rows, preferred_element_type=F32)
         out_moe[...] = total.astype(BF16)
 
+    mid_y, mid_t = (ny + 1) // 2, (tp_n // 2 + 1) // 2 * 2
     moe = [
         moe_arrive,
         moe_gather_relay,
         moe_gather_turn,
         moe_gather_relay2,
-        lambda: (moe_hidden(), moe_down()),
+        lambda: (moe_gathered(), moe_hidden(range(mid_y))),
+        lambda: (moe_hidden(range(mid_y, ny)), moe_act()),
+        lambda: (loads[7].wait(), moe_down(0, mid_t)),
+        lambda: (moe_down(mid_t, tp_n), expert_sum[0]()),
         expert_sum[1],
         expert_sum[2],
         expert_sum[3],
         expert_sum[4],
         moe_combine,
     ]
+    moe_at = list(moe_at)
+    assert len(moe_at) == len(moe)
 
     def moe_slot(number):
-        while moe_at and moe and moe_at[0] <= number:
+        while moe_at and moe_at[0] <= number:
             moe_at.pop(0)
             moe.pop(0)()
-
-    moe_at = list(moe_at)
 
     cross["k", 0].wait_recv()
     cross["v", 0].wait_recv()
@@ -554,10 +584,6 @@
     landed(half)
     attend_up(half)
 
-    @pl.when(z < half)
-    def _():
-        pass
-
     att[...] = (acc[:, 0:LANES] / acc[:, LANES:]).astype(BF16)
 
     def mix_done(first, second):
@@ -567,12 +593,10 @@
     mix = SumPlane(links, nx, ny, x, y, at_x, at_y, mix_part, mix_bufs).steps(mix_done)
     loads[8].wait()
     project(att[...], mixw, mix_part)
-    mix.pop(0)()
-    while mix or moe:
-        if moe:
-            moe.pop(0)()
-        if mix:
-            mix.pop(0)()
+    for k, step in enumerate(mix):
+        step()
+        moe_slot(100 + k)
+    moe_slot(1000)
     links.finish()
     each_peer(lambda o: dispatch_copy(o).wait_send())
     each_peer(lambda o: return_copy(o).wait_send())
@@ -587,19 +611,17 @@
     slots = -(-cap // 16) * 16
     hidden = gate_weight.shape[2]
     held = experts * cap
-    route_weight = group_gate[:, None] * inner_gate / jnp.sum(inner_gate, axis=1, keepdims=True)
-    gates = log_gate_sums.reshape(nz, 2 * rows_a)
 
     def v(*shape, dtype=BF16):
         return pltpu.VMEM(shape, dtype)
 
     scratch = [
-        v(nz, 2 * rows_a, LANES), v(nz, 2 * rows_a, LANES), v(rows_a, LANES), v(nz, 2 * rows_a, dtype=F32),
+        v(nz, 2 * rows_a, LANES), v(nz, 2 * rows_a, LANES), v(rows_a, LANES), v(1, nz * 2 * rows_a, dtype=F32),
         v(rows_a, 2 * LANES, dtype=F32), v(rows_a, LANES, dtype=F32),
         v(LANES, width), v(ny, nx, rows_a, LANES), v(rows_a, LANES),
         v(rows_m, width), v(width, hidden), v(width, hidden), v(hidden, width),
         v(experts, slots, LANES), v(experts, slots, LANES), v(ny, nx, held, LANES), v(ny, nx, held, LANES),
-        v(experts, slots, LANES), v(experts, slots, LANES),
+        v(experts, slots, LANES), v(experts, slots, LANES), v(LANES, -(-rows_m // LANES) * LANES, dtype=F32),
         pltpu.SemaphoreType.DMA((SEM_LIMIT,)),
         pltpu.SemaphoreType.DMA((2 * nz,)), pltpu.SemaphoreType.DMA((2 * nz,)),
         pltpu.SemaphoreType.DMA((2 * nz,)), pltpu.SemaphoreType.DMA((2 * nz,)),
@@ -623,12 +645,12 @@
         ),
         name="step",
     )(
-        queries, keys, values, gates, mixer_weight, moe_rows, route_ids, route_ids.T, route_weight,
-        norm_gain.reshape(1, -1), gate_weight[0], up_weight[0], down_weight[0],
-    )
-
-
-MOE_AT = (5, 6, 7, 9, 11, 14, 16)
+        queries, keys, values, log_gate_sums.T, mixer_weight, moe_rows, route_ids.T,
+        group_gate.reshape(1, -1), inner_gate.T, norm_gain.reshape(1, -1), gate_weight[0], up_weight[0], down_weight[0],
+    )
+
+
+MOE_AT = (3, 4, 5, 7, 9, 9, 10, 11, 13, 15, 16, 100, 103)
 
 
 def plane_of(tp):

time: 122 us -> 101 us (0.83)
  the two profiles are of different devices: /device:TPU:1 before, /device:TPU:32 now
where the time goes in v2:
time: 101 us
  Pallas kernels  98 us (97%)
  local copies, waits for them, and re-layouts  2.2 us (2%)
    pallas_call x1, Pallas kernels, body(): pl.pallas_call(functools.partial(kernel, (nz, nx, ny, cap, slots, moe_at)...  98 us
    unnamed x4, local copies, waits for them, and re-layouts  2.2 us

profile of v2, /device:TPU:32, one launch (start us, length us, event | category | flops | bytes accessed | tf_op | source)
XLA Modules:
  0.0 100.8 jit_solution(2108113952235914942)
XLA Ops:
  0.6 98.0 %step.1 = (bf16[512,128]{1,0:T(8,128)(2,1)}, bf16[192,128]{1,0:T(8,128)(2,1)}) custom-call(bf16[512,128]{1,0:T(8,128)(2,1)} %refs_0_.1, bf16[512,128]{1,0:T(8,128)(2,1)} %refs_1_.1, bf16[512,128]{1,0:T(8,128)(2,1)} %refs_2_.1, f32[1,16384]{1,0:T(1,128)} %bitcast.11, bf16[128,2048]{1,0:T(8,128)(2,1)} %refs_4_.1, bf16[192,2048]{1,0:T(8,128)(2,1)} %refs_5_.1, ...), custom_call_target="tpu_custom_call" | custom-call | tf_op jit(solution)/shard_map/step/pallas_call | solution.py:634
  98.6 0.0 copy-start
  98.6 1.6 %copy.17 = bf16[512,128]{1,0:T(8,128)(2,1)} copy(bf16[512,128]{1,0:T(8,128)(2,1)} %get-tuple-element.4) | data formatting | bytes 262144
  100.2 0.0 copy-done
  100.2 0.6 copy.18
Async XLA Ops:
  98.6 1.6 %copy-start = (bf16[192,128]{1,0:T(8,128)(2,1)S(1)}, bf16[192,128]{1,0:T(8,128)(2,1)}, u32[]{:S(2)}) copy-start(bf16[192,128]{1,0:T(8,128)(2,1)} %get-tuple-element.5) | copy-start | bytes 147460

commit v3 on v2

--- a/solution.py
+++ b/solution.py
@@ -84,13 +84,16 @@
             self.down[0].wait_recv()
             self.links.start(self.relay_down)
 
-    def end(self):
+    def near(self):
         if self.n == 2:
             self.up[0].wait_recv()
             self.up[1].wait_recv()
         if self.n == 4:
             self.up[1].wait_recv()
             self.down[1].wait_recv()
+
+    def end(self):
+        if self.n == 4:
             self.relay_up.wait_recv()
             self.relay_down.wait_recv()
 
@@ -123,6 +126,18 @@
             self.links.start(self.up_plain)
             self.links.start(self.up)
 
+    def begin_part(self, offset):
+        if self.n == 4 and offset == 2:
+            self.links.start(self.far_up)
+            self.links.start(self.far_down)
+        if self.n == 4 and offset == 1:
+            self.links.start(self.up_plain)
+        if self.n == 4 and offset == 3:
+            self.links.start(self.down_plain)
+        if self.n == 2 and offset == 1:
+            self.links.start(self.up_plain)
+            self.links.start(self.up)
+
     def relay(self):
         if self.n == 4:
             self.far_up.wait_recv()
@@ -147,58 +162,68 @@
         return total
 
 
+def spread_order(n):
+    return {4: (2, 1, 3, 0), 2: (1, 0), 1: (0,)}[n]
+
+
 class SumPlane:
 
     def __init__(self, links, nx, ny, x, y, at_x, at_y, part, bufs):
         rows = part.shape[2]
         h = rows // 2
         q = h // 2
-        (ha, hb, fa, fb, sa, ga, gb, ea, eb) = bufs[:9]
-        (hc, hd, fc, fd, sb, gc, gd, ec, ed) = bufs[9:]
-        self.sa, self.sb = sa, sb
-
-        def wide_first(r):
-            return r.at[:, pl.ds(0, q), :]
-
-        def wide_second(r):
-            return r.at[:, pl.ds(q, q), :]
-
-        def flat_first(r):
+
+        def first(r):
             return r.at[pl.ds(0, q), :]
 
-        def flat_second(r):
+        def second(r):
             return r.at[pl.ds(q, q), :]
 
-        self.a1 = SumLine(
-            links, nx, x, at_x, lambda c: part.at[:, c, pl.ds(0, h), :], wide_first, wide_second, ha, hb, fa, fb
-        )
-        self.b1 = SumLine(
-            links, ny, y, at_y, lambda c: part.at[c, :, pl.ds(h, h), :], wide_first, wide_second, hc, hd, fc, fd
-        )
-        self.a2 = SumLine(links, ny, y, at_y, lambda c: sa.at[c], flat_first, flat_second, ga, gb, ea, eb)
-        self.b2 = SumLine(links, nx, x, at_x, lambda c: sb.at[c], flat_first, flat_second, gc, gd, ec, ed)
+        def way(n1, c1, at1, n2, c2, at2, block, buf):
+            (ha, hb, fa, fb, mid, ga, gb, ea, eb) = buf
+            lines = []
+            for k, o in enumerate(spread_order(n2)):
+                other = (c2 + o) % n2
+                line = SumLine(
+                    links, n1, c1, at1, functools.partial(block, other), first, second,
+                    ha.at[k], hb.at[k], fa.at[k], fb.at[k],
+                )
+                lines.append((o, other, line))
+            last = SumLine(links, n2, c2, at2, lambda c: mid.at[c], first, second, ga, gb, ea, eb)
+            return lines, mid, last
+
+        self.ways = [
+            way(nx, x, at_x, ny, y, at_y, lambda other, c: part.at[other, c, pl.ds(0, h), :], bufs[:9]),
+            way(ny, y, at_y, nx, x, at_x, lambda other, c: part.at[c, other, pl.ds(h, h), :], bufs[9:]),
+        ]
 
     def steps(self, done):
         def begin():
-            self.a1.begin()
-            self.b1.begin()
+            for k in range(max(len(w[0]) for w in self.ways)):
+                for lines, _, _ in self.ways:
+                    if k < len(lines):
+                        lines[k][2].begin()
 
         def relay():
-            self.a1.relay()
-            self.b1.relay()
+            for k in range(max(len(w[0]) for w in self.ways)):
+                for lines, _, _ in self.ways:
+                    if k < len(lines):
+                        lines[k][2].relay()
 
         def turn():
-            self.sa[...] = self.a1.end().astype(BF16)
-            self.a2.begin()
-            self.sb[...] = self.b1.end().astype(BF16)
-            self.b2.begin()
+            for k in range(max(len(w[0]) for w in self.ways)):
+                for lines, mid, last in self.ways:
+                    if k < len(lines):
+                        o, other, line = lines[k]
+                        mid[other] = line.end().astype(BF16)
+                        last.begin_part(o)
 
         def relay2():
-            self.a2.relay()
-            self.b2.relay()
+            for _, _, last in self.ways:
+                last.relay()
 
         def end():
-            done(self.a2.end(), self.b2.end())
+            done(*[last.end() for _, _, last in self.ways])
 
         return [begin, relay, turn, relay2, end]
 
@@ -216,7 +241,7 @@
     ]
 
 
-SEM_LIMIT = 300
+SEM_LIMIT = 500
 
 
 def kernel(cfg, *refs):
@@ -399,7 +424,7 @@
     def attend(chip, masked):
         bias = (gates_of(chip, 0, chunk) - base) * LOG2E
         ones = jnp.ones((chunk, LANES), BF16)
-        for i in range(rows_a // q_block):
+        def query_rows(i):
             here = pl.ds(i * q_block, q_block)
             scores = (
                 lax.dot_general(
@@ -421,6 +446,9 @@
             add = jnp.dot(weights, both, preferred_element_type=F32)
             acc[here, :] = acc[here, :] * jnp.concatenate([shrink, shrink], axis=1) + add
 
+        for i in range(rows_a // q_block):
+            query_rows(i)
+
     gather = {}
     h, qtr = held // 2, held // 4
     gather["a1"] = GatherLine(
@@ -431,14 +459,27 @@
         links, ny, y, at_y, lambda c: feats.at[c, x, pl.ds(h, h), :],
         lambda r: r.at[pl.ds(0, qtr), :], lambda r: r.at[pl.ds(qtr, qtr), :],
     )
-    gather["a2"] = GatherLine(
-        links, ny, y, at_y, lambda c: feats.at[c, :, pl.ds(0, h), :],
-        lambda r: r.at[:, pl.ds(0, qtr), :], lambda r: r.at[:, pl.ds(qtr, qtr), :],
-    )
-    gather["b2"] = GatherLine(
-        links, nx, x, at_x, lambda c: feats.at[:, c, pl.ds(h, h), :],
-        lambda r: r.at[:, pl.ds(0, qtr), :], lambda r: r.at[:, pl.ds(qtr, qtr), :],
-    )
+
+    def upper(r):
+        return r.at[pl.ds(0, qtr), :]
+
+    def lower(r):
+        return r.at[pl.ds(qtr, qtr), :]
+
+    def second_line(n1, c1, n2, c2, dev, block):
+        lines = {}
+        for o in range(n1):
+            lines[o] = GatherLine(links, n2, c2, dev, functools.partial(block, (c1 + o) % n1), upper, lower)
+        return lines
+
+    gather["a2"] = second_line(nx, x, ny, y, at_y, lambda other, c: feats.at[c, other, pl.ds(0, h), :])
+    gather["b2"] = second_line(ny, y, nx, x, at_x, lambda other, c: feats.at[other, c, pl.ds(h, h), :])
+
+    def second_stage(offsets, do):
+        for o in offsets:
+            for key in ("a2", "b2"):
+                if o in gather[key]:
+                    do(gather[key][o])
 
     def packed_row(shape, dim):
         i = lax.broadcasted_iota(jnp.int32, shape, dim)
@@ -453,26 +494,33 @@
         ).astype(BF16)
         gather["a1"].begin()
         gather["b1"].begin()
+        second_stage((0,), GatherLine.begin)
+
+    def near_offsets(n):
+        return {4: (1, 3), 2: (1,), 1: ()}[n]
 
     def moe_gather_relay():
         gather["a1"].relay()
         gather["b1"].relay()
+        for key, n in (("a", nx), ("b", ny)):
+            gather[key + "1"].near()
+            for o in near_offsets(n):
+                gather[key + "2"][o].begin()
 
     def moe_gather_turn():
-        gather["a1"].end()
-        gather["a2"].begin()
-        gather["b1"].end()
-        gather["b2"].begin()
+        for key, n in (("a", nx), ("b", ny)):
+            gather[key + "1"].end()
+            if n == 4:
+                gather[key + "2"][2].begin()
+        second_stage((0,), GatherLine.relay)
 
     def moe_gather_relay2():
-        gather["a2"].relay()
-        gather["b2"].relay()
+        second_stage((1, 3, 2), GatherLine.relay)
 
     made = {"gate": 0.0, "up": 0.0}
 
     def moe_gathered():
-        gather["a2"].end()
-        gather["b2"].end()
+        second_stage((0, 1, 3, 2), lambda line: (line.near(), line.end()))
         loads[5].wait()
         loads[6].wait()
 
@@ -573,14 +621,16 @@
 
     for d in range(1, half + 1):
         pass_on("k", d)
+        moe_slot(4 * d - 3)
         if d > 1:
             landed(d - 1)
             attend_up(d - 1)
-        moe_slot(2 * d - 1)
+        moe_slot(4 * d - 2)
         pass_on("v", d)
+        moe_slot(4 * d - 1)
         if d > 1:
             attend_down(d - 1)
-        moe_slot(2 * d)
+        moe_slot(4 * d)
     landed(half)
     attend_up(half)
 
@@ -634,8 +684,8 @@
     return pl.pallas_call(
         functools.partial(kernel, (nz, nx, ny, cap, slots, moe_at)),
         out_shape=(
-            jax.ShapeDtypeStruct((rows_a, LANES), BF16),
-            jax.ShapeDtypeStruct((rows_m, LANES), BF16),
+            pltpu.VMEM((rows_a, LANES), BF16),
+            pltpu.VMEM((rows_m, LANES), BF16),
         ),
         in_specs=[hbm] * 6 + [vm] * 4 + [hbm] * 3,
         out_specs=(vm, vm),
@@ -650,7 +700,7 @@
     )
 
 
-MOE_AT = (3, 4, 5, 7, 9, 9, 10, 11, 13, 15, 16, 100, 103)
+MOE_AT = (6, 8, 9, 12, 16, 17, 18, 20, 24, 28, 32, 100, 103)
 
 
 def plane_of(tp):

time: 101 us -> 97.8 us (0.968)
  the two profiles are of different devices: /device:TPU:32 before, /device:TPU:1 now
where the time goes in v3:
time: 97.8 us; the launch traced here: 97.7 us
  Pallas kernels  95.8 us (98%)
  local copies, waits for them, and re-layouts  1.28 us (1%)
    pallas_call x1, Pallas kernels, body(): pl.pallas_call(functools.partial(kernel, (nz, nx, ny, cap, slots, moe_at)...  95.8 us

profile of v3, /device:TPU:1, one launch (start us, length us, event | category | flops | bytes accessed | tf_op | source)
XLA Modules:
  0.0 97.7 jit_solution(16206496298129198514)
XLA Ops:
  0.6 95.8 %step.1 = (bf16[512,128]{1,0:T(8,128)(2,1)S(1)}, bf16[192,128]{1,0:T(8,128)(2,1)S(1)}) custom-call(bf16[512,128]{1,0:T(8,128)(2,1)} %refs_0_.1, bf16[512,128]{1,0:T(8,128)(2,1)} %refs_1_.1, bf16[512,128]{1,0:T(8,128)(2,1)} %refs_2_.1, f32[1,16384]{1,0:T(1,128)} %bitcast.11, bf16[128,2048]{1,0:T(8,128)(2,1)} %refs_4_.1, bf16[192,2048]{1,0:T(8,128)(2,1)} %refs_5_.1, ...), custom_call_target="tpu_custom_call" | custom-call | tf_op jit(solution)/shard_map/step/pallas_call | solution.py:684
  96.4 0.7 copy.17
  97.1 0.6 copy.18
